TPU v7x, 32 devices: a whole 2x2x4 slice. The times are simulated.
32 devices in a mesh: sp: 16 (over z, y, x), tp: 2 (over core).
Axes of the slice: x: 2, y: 2, z: 4, core: 2. Of those that a mesh axis runs over, the one named last changes fastest.
Arguments:
- tokens: bfloat16 [2048, 1024], P('sp', 'tp'), may hold values from -6 to 6
- norm_gain: float32 [1024], P('tp'), may hold values from 0.1 to 1.9
- query_weight: bfloat16 [1024, 1024], P('sp', 'tp'), may hold values from -0.1875 to 0.1875
- key_weight: bfloat16 [1024, 512], P('sp', 'tp'), may hold values from -0.1875 to 0.1875
- value_weight: bfloat16 [1024, 512], P('sp', 'tp'), may hold values from -0.1875 to 0.1875
- conv_in_weight: bfloat16 [1024, 1024], P('sp', 'tp'), may hold values from -0.1875 to 0.1875
- pre_weight: bfloat16 [1024, 1024], P('sp', 'tp'), may hold values from -0.1875 to 0.1875
- post_weight: bfloat16 [1024, 1024], P('sp', 'tp'), may hold values from -0.1875 to 0.1875
- attn_gate_weight: bfloat16 [1024, 1024], P('sp', 'tp'), may hold values from -0.1875 to 0.1875
- conv_gate_weight: bfloat16 [1024, 1024], P('sp', 'tp'), may hold values from -0.1875 to 0.1875
- sink_logit: float32 [16], P('tp'), may hold values from 1 to 5
- conv_taps: float32 [3, 1024], P(None, 'tp'), may hold values from -3 to 3
- attn_out_weight: bfloat16 [1024, 1024], P('tp', 'sp'), may hold values from -1 to 1
- conv_out_weight: bfloat16 [1024, 1024], P('tp', 'sp'), may hold values from -0.1875 to 0.1875
Outputs:
- merged: bfloat16 [2048, 1024], P('sp', 'tp')
All inputs are finite; a program needn't handle non-finite values.
Results may differ from a plain program's by a relative error of at most 0.003.
Values may be sent and summed in bfloat16 or wider, within the bound.
A program may use at most 64 MiB of HBM per device.

v0:
```python
import jax
import jax.numpy as jnp
from jax import lax
from jax.sharding import PartitionSpec as P

HEAD_DIM = 64
WINDOW = 64
epsilon = 1e-06
negative = -1e30


def folded(shard, axis, dim, absorb, state):
    everything = jax.tree.map(lambda a: lax.all_gather(a, axis, axis=dim, tiled=True), shard)
    return absorb(state, everything, jnp.int32(0))


def for_sending(shard):

    def short(part):
        return part.astype(jnp.bfloat16) if part.dtype == jnp.float32 else part

    return jax.tree.map(short, shard)


def extended(shard, sides, width, wrap):
    for axis, dim in sides:
        devices, length = (lax.axis_size(axis), shard.shape[dim])
        up = [(i, (i + 1) % devices) for i in range(devices if wrap else devices - 1)]
        down = [(j, i) for i, j in up]
        last = lax.slice_in_dim(shard, length - width, length, axis=dim)
        first = lax.slice_in_dim(shard, 0, width, axis=dim)
        before = lax.ppermute(last, axis, up)
        after = lax.ppermute(first, axis, down)
        shard = jnp.concatenate([before, shard, after], axis=dim)
    return shard


def summed_rows(product, width, axis):
    whole = product(jnp.int32(0), width * lax.axis_size(axis))
    return lax.psum_scatter(whole, axis, scatter_dimension=0, tiled=True)


def window_mix(queries, key_rows, value_rows, sink_cols, first, seq_total):
    score_scale = queries.shape[-1] ** (-0.5)
    scores = (
        jnp.einsum("qhgd,khd->hgqk", queries, key_rows, preferred_element_type=jnp.float32)
        * score_scale
    )
    qpos = first + jnp.arange(queries.shape[0], dtype=jnp.int32)
    kpos = first - WINDOW + jnp.arange(key_rows.shape[0], dtype=jnp.int32)
    allowed = (
        (jnp.abs(qpos[:, None] - kpos[None, :]) <= WINDOW)
        & (kpos >= 0)[None, :]
        & (kpos < seq_total)[None, :]
    )
    scores = jnp.where(allowed, scores, negative)
    column = jnp.broadcast_to(sink_cols[:, :, None, None], scores.shape[:-1] + (1,))
    weights_soft = jax.nn.softmax(jnp.concatenate([scores, column], axis=-1), axis=-1)[..., :-1]
    return jnp.einsum(
        "hgqk,khd->qhgd",
        weights_soft,
        value_rows.astype(jnp.float32),
        precision=lax.Precision.HIGHEST,
    )


def short_conv(padded, conv_taps):
    return (
        conv_taps[0][None, :] * padded[:-2]
        + conv_taps[1][None, :] * padded[1:-1]
        + conv_taps[2][None, :] * padded[2:]
    )


def per_device(
    tokens,
    norm_gain,
    query_weight,
    key_weight,
    value_weight,
    conv_in_weight,
    pre_weight,
    post_weight,
    attn_gate_weight,
    conv_gate_weight,
    sink_logit,
    conv_taps,
    attn_out_weight,
    conv_out_weight,
):
    tok_rows = tokens.shape[0]
    widened = tokens.astype(jnp.float32)
    row_sums = lax.psum(jnp.sum(widened * widened, axis=1), "tp")
    features = tokens.shape[1] * lax.axis_size("tp")
    normed = (
        widened * lax.rsqrt(row_sums[:, None] / features + epsilon) * norm_gain[None, :]
    ).astype(jnp.bfloat16)
    collected = (
        lax.all_gather(query_weight, "sp", axis=0, tiled=True),
        lax.all_gather(key_weight, "sp", axis=0, tiled=True),
        lax.all_gather(value_weight, "sp", axis=0, tiled=True),
        lax.all_gather(conv_in_weight, "sp", axis=0, tiled=True),
        lax.all_gather(pre_weight, "sp", axis=0, tiled=True),
        lax.all_gather(post_weight, "sp", axis=0, tiled=True),
        lax.all_gather(attn_gate_weight, "sp", axis=0, tiled=True),
        lax.all_gather(conv_gate_weight, "sp", axis=0, tiled=True),
    )
    stacked = jnp.concatenate(collected, axis=1)

    def add_rows(carry_sum, segment, first):
        rows_here = lax.dynamic_slice_in_dim(stacked, first, segment.shape[1], 0)
        return carry_sum + jnp.dot(segment, rows_here, preferred_element_type=jnp.float32)

    projected = folded(
        normed, "tp", 1, add_rows, jnp.zeros((tok_rows, stacked.shape[1]), jnp.float32)
    )
    pieces = []
    offset = 0
    for weight in collected:
        pieces.append(projected[:, offset : offset + weight.shape[1]])
        offset = offset + weight.shape[1]
    queries, key_rows, value_rows, conv_in, pre_gate, post_gate = [
        part_rows.astype(jnp.bfloat16) for part_rows in pieces[:6]
    ]
    attn_gate = pieces[6]
    conv_gate = pieces[7]
    conv_mix = (pre_gate.astype(jnp.float32) * conv_in.astype(jnp.float32)).astype(jnp.bfloat16)
    kv_width = key_rows.shape[1]
    kv_pad = extended(
        for_sending(jnp.concatenate([key_rows, value_rows], axis=1)), (("sp", 0),), WINDOW, False
    )
    key_pad = kv_pad[:, :kv_width]
    value_pad = kv_pad[:, kv_width:]
    conv_pad = extended(conv_mix, (("sp", 0),), 1, False)
    kv_local = kv_width // HEAD_DIM
    group_size = queries.shape[1] // kv_width
    first_row = lax.axis_index("sp") * tok_rows
    attended = window_mix(
        queries.reshape(tok_rows, kv_local, group_size, HEAD_DIM),
        key_pad.reshape(-1, kv_local, HEAD_DIM),
        value_pad.reshape(-1, kv_local, HEAD_DIM),
        sink_logit.reshape(kv_local, group_size),
        first_row,
        tok_rows * lax.axis_size("sp"),
    )
    attended = attended.reshape(tok_rows, -1).astype(jnp.bfloat16)
    conv_out = (
        post_gate.astype(jnp.float32) * short_conv(conv_pad.astype(jnp.float32), conv_taps)
    ).astype(jnp.bfloat16)
    attn_full, conv_full = (
        lax.all_gather(attn_out_weight, "sp", axis=1, tiled=True),
        lax.all_gather(conv_out_weight, "sp", axis=1, tiled=True),
    )

    def attn_term(first, number):
        columns = lax.dynamic_slice_in_dim(attn_full, first, number, 1)
        return jnp.dot(attended, columns, preferred_element_type=jnp.float32).T

    def conv_term(first, number):
        columns = lax.dynamic_slice_in_dim(conv_full, first, number, 1)
        return jnp.dot(conv_out, columns, preferred_element_type=jnp.float32).T

    out_rows = attn_gate.shape[1]

    def both_terms(first, number):
        return jnp.concatenate([attn_term(first, number), conv_term(first, number)], axis=1)

    summed = summed_rows(both_terms, out_rows, "tp")
    branch_attn = summed[:, :tok_rows].T
    branch_conv = summed[:, tok_rows:].T
    return (
        jax.nn.sigmoid(attn_gate) * branch_attn + jax.nn.sigmoid(conv_gate) * branch_conv
    ).astype(jnp.bfloat16)


def solution(mesh):
    return jax.shard_map(
        per_device,
        mesh=mesh,
        in_specs=(
            P("sp", "tp"),
            P("tp"),
            P("sp", "tp"),
            P("sp", "tp"),
            P("sp", "tp"),
            P("sp", "tp"),
            P("sp", "tp"),
            P("sp", "tp"),
            P("sp", "tp"),
            P("sp", "tp"),
            P("tp"),
            P(None, "tp"),
            P("tp", "sp"),
            P("tp", "sp"),
        ),
        out_specs=P("sp", "tp"),
        check_vma=False,
    )
```

profile of v0, /device:TPU:0, one launch (start us, length us, event | category | flops | bytes accessed | tf_op | source)
XLA Modules:
  0.0 485.7 jit_solution(2736074384034451135)
XLA Ops:
  6.5 0.7 all-gather.9.cloned.1.call-update
  7.3 0.0 all-gather.11.cloned.1.call-start
  7.3 0.7 all-gather.11.cloned.1.call-update
  8.0 0.0 all-gather.13.cloned.1.call-start
  8.1 0.7 all-gather.13.cloned.1.call-update
  8.7 0.0 all-gather.15.cloned.1.call-start
  8.8 0.5 all-gather.15.cloned.1.call-update
  9.3 0.0 all-gather.17.cloned.1.call-start
  9.4 0.5 all-gather.17.cloned.1.call-update
  9.9 0.0 all-gather.19.cloned.1.call-start
  9.9 0.5 all-gather.19.cloned.1.call-update
  10.5 0.0 all-gather.23.cloned.1.call-start
  10.5 0.7 all-gather.23.cloned.1.call-update
  11.2 0.0 all-gather.21.cloned.1.call-start
  11.3 0.7 all-gather.21.cloned.1.call-update
  12.0 0.0 reduce-scatter.2.cloned.1.call-start
  12.1 45.7 %all_gather.35 = bf16[1024,256]{1,0:T(8,128)(2,1)S(1)} all-gather(bf16[64,256]{1,0:T(8,128)(2,1)} %param.17), channel_id=1, replica_groups=mesh['sp'=16,'tp'=2] {'sp'}, dimensions={0}, use_global_device_ids=true | all-gather | bytes 557056 | tf_op jit(solution)/shard_map/all_gather | solution.py:100
  57.8 40.3 %all_gather.36 = bf16[1024,256]{1,0:T(8,128)(2,1)S(1)} all-gather(bf16[64,256]{1,0:T(8,128)(2,1)} %param.18), channel_id=1, replica_groups=mesh['sp'=16,'tp'=2] {'sp'}, dimensions={0}, use_global_device_ids=true | all-gather | bytes 557056 | tf_op jit(solution)/shard_map/all_gather | solution.py:101
  98.1 1.0 fusion.4
  99.1 2.5 psum.7
  101.6 1.0 fusion.6
  102.6 2.0 all_gather.33
  104.6 1.3 broadcast_in_dim.27
  105.9 1.4 fusion.35
  107.3 0.8 fusion.27
  108.1 2.3 constant_dynamic-update-slice_fusion.7
  110.4 0.9 constant_dynamic-update-slice_fusion.6
  111.3 0.9 constant_dynamic-update-slice_fusion.5
  112.2 15.1 %all-gather.11.cloned.1.call-done = bf16[1024,512]{1,0:T(8,128)(2,1)} async-done(((bf16[64,512]{1,0:T(8,128)(2,1)}), bf16[1024,512]{1,0:T(8,128)(2,1)}) %all-gather.11.cloned.1.call-update) | async-done | bytes 1048592 | tf_op jit(solution)/shard_map/all_gather | solution.py:102
  127.3 2.3 constant_dynamic-update-slice_fusion.4
  129.6 54.4 %all-gather.13.cloned.1.call-done = bf16[1024,512]{1,0:T(8,128)(2,1)} async-done(((bf16[64,512]{1,0:T(8,128)(2,1)}), bf16[1024,512]{1,0:T(8,128)(2,1)}) %all-gather.13.cloned.1.call-update) | async-done | bytes 1048592 | tf_op jit(solution)/shard_map/all_gather | solution.py:103
  184.0 2.3 constant_dynamic-update-slice_fusion.3
  186.3 54.3 %all-gather.15.cloned.1.call-done = bf16[1024,512]{1,0:T(8,128)(2,1)} async-done(((bf16[64,512]{1,0:T(8,128)(2,1)}), bf16[1024,512]{1,0:T(8,128)(2,1)}) %all-gather.15.cloned.1.call-update) | async-done | bytes 1048592 | tf_op jit(solution)/shard_map/all_gather | solution.py:104
  240.6 2.3 constant_dynamic-update-slice_fusion.2
  242.9 54.2 %all-gather.17.cloned.1.call-done = bf16[1024,512]{1,0:T(8,128)(2,1)} async-done(((bf16[64,512]{1,0:T(8,128)(2,1)}), bf16[1024,512]{1,0:T(8,128)(2,1)}) %all-gather.17.cloned.1.call-update) | async-done | bytes 1048592 | tf_op jit(solution)/shard_map/all_gather | solution.py:105
  297.1 2.3 constant_dynamic-update-slice_fusion.1
  299.5 54.2 %all-gather.19.cloned.1.call-done = bf16[1024,512]{1,0:T(8,128)(2,1)} async-done(((bf16[64,512]{1,0:T(8,128)(2,1)}), bf16[1024,512]{1,0:T(8,128)(2,1)}) %all-gather.19.cloned.1.call-update) | async-done | bytes 1048592 | tf_op jit(solution)/shard_map/all_gather | solution.py:106
  353.7 2.3 constant_dynamic-update-slice_fusion
  356.0 4.2 fusion.36
  360.3 0.7 fusion.31
  361.0 3.3 collective-permute-start.2
  364.3 1.3 collective-permute-start.3
  365.6 0.7 fusion.32
  366.3 5.2 %collective-permute-start = (bf16[64,512]{1,0:T(8,128)(2,1)}, bf16[64,512]{1,0:T(8,128)(2,1)}, u32[]{:S(2)}, u32[]{:S(2)}) collective-permute-start(bf16[64,512]{1,0:T(8,128)(2,1)} %get-tuple-element.9), channel_id=1, source_target_pairs={{0,2},{2,4},{4,6},{6,8},{8,10},{10,12},{12,14},{14,16},{16,18},{18... | collective-permute-start | bytes 196616 | tf_op jit(solution)/shard_map/ppermute | solution.py:32
  371.5 1.3 collective-permute-start.1
  372.7 0.7 copy.21
  373.5 0.0 collective-permute-done.2
  373.5 0.0 collective-permute-done.3
  373.5 36.9 %all-gather.23.cloned.1.call-done = bf16[512,1024]{0,1:T(8,128)(2,1)} async-done(((bf16[512,64]{0,1:T(8,128)(2,1)}), bf16[512,1024]{0,1:T(8,128)(2,1)}) %all-gather.23.cloned.1.call-update) | async-done | bytes 1048592 | tf_op jit(solution)/shard_map/all_gather | solution.py:152
  410.5 1.7 convolution_bitcast_fusion
  412.2 1.0 pad_maximum_fusion.1
  413.2 0.1 copy.20
  413.3 0.1 copy.19
  413.4 1.3 fusion.37
  414.7 0.7 broadcast_maximum_fusion
  415.4 0.7 broadcast_in_dim.28
  416.2 0.2 fusion.30
  416.3 0.6 convolution_convert_fusion
  416.9 50.3 %all-gather.21.cloned.1.call-done = bf16[512,1024]{0,1:T(8,128)(2,1)} async-done(((bf16[512,64]{0,1:T(8,128)(2,1)}), bf16[512,1024]{0,1:T(8,128)(2,1)}) %all-gather.21.cloned.1.call-update) | async-done | bytes 1048592 | tf_op jit(solution)/shard_map/all_gather | solution.py:151
  467.2 1.7 convolution_bitcast_fusion.1
  468.9 1.1 pad_maximum_fusion
  469.9 0.0 reduce-scatter.2.cloned.1.call-update
  470.0 7.4 %reduce-scatter.2.cloned.1.call-done = f32[512,256]{0,1:T(8,128)} async-done(((f32[1024,256]{0,1:T(8,128)}), f32[512,256]{0,1:T(8,128)}) %reduce-scatter.2.cloned.1.call-update) | async-done | bytes 524304 | tf_op jit(solution)/shard_map/reduce_scatter | solution.py:40
  477.3 1.8 fusion.9
  (12 shorter events, 0.1 us)
Async XLA Ops:
  6.5 101.6 %all-gather.9.cloned.1.call-start = ((), (), s32[]{:S(2)}) async-start(), calls=%async_computation.1 | async-start | bytes 1114112 | tf_op jit(solution)/shard_map/all_gather | solution.py:99
  7.3 120.0 %all-gather.11.cloned.1.call-start = ((), (), s32[]{:S(2)}) async-start(), calls=%async_computation.2 | async-start | bytes 1114112 | tf_op jit(solution)/shard_map/all_gather | solution.py:102
  8.0 176.0 %all-gather.13.cloned.1.call-start = ((), (), s32[]{:S(2)}) async-start(), calls=%async_computation.3 | async-start | bytes 1114112 | tf_op jit(solution)/shard_map/all_gather | solution.py:103
  8.7 231.8 %all-gather.15.cloned.1.call-start = ((), (), s32[]{:S(2)}) async-start(), calls=%async_computation.4 | async-start | bytes 1114112 | tf_op jit(solution)/shard_map/all_gather | solution.py:104
  9.3 287.8 %all-gather.17.cloned.1.call-start = ((), (), s32[]{:S(2)}) async-start(), calls=%async_computation.5 | async-start | bytes 1114112 | tf_op jit(solution)/shard_map/all_gather | solution.py:105
  9.9 343.8 %all-gather.19.cloned.1.call-start = ((), (), s32[]{:S(2)}) async-start(), calls=%async_computation.6 | async-start | bytes 1114112 | tf_op jit(solution)/shard_map/all_gather | solution.py:106
  10.5 400.0 %all-gather.23.cloned.1.call-start = ((), (), s32[]{:S(2)}) async-start(), calls=%async_computation.8 | async-start | bytes 1114112 | tf_op jit(solution)/shard_map/all_gather | solution.py:152
  11.2 455.9 %all-gather.21.cloned.1.call-start = ((), (), s32[]{:S(2)}) async-start(), calls=%async_computation.7 | async-start | bytes 1114112 | tf_op jit(solution)/shard_map/all_gather | solution.py:151
  12.0 465.4 %reduce-scatter.2.cloned.1.call-start = ((), (), s32[]{:S(2)}) async-start(), calls=%async_computation.9 | async-start | bytes 1572864 | tf_op jit(solution)/shard_map/reduce_scatter | solution.py:40
  361.0 12.5 %collective-permute-start.2 = (bf16[1,512]{1,0:T(2,128)(2,1)S(1)}, bf16[1,512]{1,0:T(2,128)(2,1)S(1)}, u32[]{:S(2)}, u32[]{:S(2)}) collective-permute-start(bf16[1,512]{1,0:T(2,128)(2,1)S(1)} %get-tuple-element.13), channel_id=1, source_target_pairs={{0,2},{2,4},{4,6},{6,8},{8,10},{10,12},{12,14},{14,16},{16,18},{18... | collective-permute-start | bytes 3080 | tf_op jit(solution)/shard_map/ppermute | solution.py:32
  364.3 9.2 %collective-permute-start.3 = (bf16[1,512]{1,0:T(2,128)(2,1)S(1)}, bf16[1,512]{1,0:T(2,128)(2,1)S(1)}, u32[]{:S(2)}, u32[]{:S(2)}) collective-permute-start(bf16[1,512]{1,0:T(2,128)(2,1)S(1)} %get-tuple-element.14), channel_id=1, source_target_pairs={{2,0},{4,2},{6,4},{8,6},{10,8},{12,10},{14,12},{16,14},{18,16},{20... | collective-permute-start | bytes 3080 | tf_op jit(solution)/shard_map/ppermute | solution.py:33
  366.3 45.9 %collective-permute-start = (bf16[64,512]{1,0:T(8,128)(2,1)}, bf16[64,512]{1,0:T(8,128)(2,1)}, u32[]{:S(2)}, u32[]{:S(2)}) collective-permute-start(bf16[64,512]{1,0:T(8,128)(2,1)} %get-tuple-element.9), channel_id=1, source_target_pairs={{0,2},{2,4},{4,6},{6,8},{8,10},{10,12},{12,14},{14,16},{16,18},{18... | collective-permute-start | bytes 196616 | tf_op jit(solution)/shard_map/ppermute | solution.py:32
  371.5 40.7 %collective-permute-start.1 = (bf16[64,512]{1,0:T(8,128)(2,1)}, bf16[64,512]{1,0:T(8,128)(2,1)}, u32[]{:S(2)}, u32[]{:S(2)}) collective-permute-start(bf16[64,512]{1,0:T(8,128)(2,1)} %get-tuple-element.10), channel_id=1, source_target_pairs={{2,0},{4,2},{6,4},{8,6},{10,8},{12,10},{14,12},{16,14},{18,16},{20... | collective-permute-start | bytes 196616 | tf_op jit(solution)/shard_map/ppermute | solution.py:33
Sparse Core Ops, SparseCore 0:
  10.1 59.5 all-gather.8
  72.5 54.7 all-gather.10
  130.1 53.9 all-gather.12
  186.6 53.9 all-gather.14
  243.2 53.9 all-gather.16
  299.8 53.9 all-gather.18
  356.5 53.9 all-gather.22
  413.2 53.9 all-gather.20
  470.1 7.2 reduce-scatter.1
where the time goes:
time: 486 us
  waiting for transfers between devices  332 us (68%)
  blocking collectives  90.5 us (19%)
  local copies, waits for them, and re-layouts  21.5 us (4%)
  between operations  13.4 us (3%)
  starting transfers between devices  11.4 us (2%)
  matrix products  9.44 us (2%)
  other arithmetic  7.67 us (2%)
    all_gather x1, waiting for transfers between devices, per_device(): lax.all_gather(pre_weight, 'sp', axis=0, tiled=True)  54.4 us
    all_gather x1, waiting for transfers between devices, per_device(): lax.all_gather(post_weight, 'sp', axis=0, tiled=True)  54.3 us
    all_gather x1, waiting for transfers between devices, per_device(): lax.all_gather(attn_gate_weight, 'sp', axis=0, tiled=True)  54.2 us
    all_gather x1, waiting for transfers between devices, per_device(): lax.all_gather(conv_gate_weight, 'sp', axis=0, tiled=True)  54.2 us
    all_gather x1, waiting for transfers between devices, per_device(): lax.all_gather(attn_out_weight, 'sp', axis=1, tiled=True)  50.3 us
    all_gather x1, blocking collectives, per_device(): lax.all_gather(key_weight, 'sp', axis=0, tiled=True)  45.7 us
    all_gather x1, blocking collectives, per_device(): lax.all_gather(value_weight, 'sp', axis=0, tiled=True)  40.3 us
    all_gather x1, waiting for transfers between devices, per_device(): lax.all_gather(conv_out_weight, 'sp', axis=1, tiled=True)  36.9 us
  transfers between devices with their start and end apart: 13, of which 8 were waited for; matrix products, arithmetic and copies ran while one was open for 7% of the time, Pallas kernels for 0%

commit v1 on v0

--- a/solution.py
+++ b/solution.py
@@ -7,6 +7,13 @@
 WINDOW = 64
 epsilon = 1e-06
 negative = -1e30
+
+
+def gather_over(x, axis, dim):
+    count = lax.axis_size(axis)
+    parts = jnp.stack([x for _ in range(count)])
+    parts = lax.all_to_all(parts, axis, split_axis=0, concat_axis=0)
+    return jnp.concatenate(parts, axis=dim)
 
 
 def folded(shard, axis, dim, absorb, state):
@@ -103,7 +110,7 @@
         lax.all_gather(pre_weight, "sp", axis=0, tiled=True),
         lax.all_gather(post_weight, "sp", axis=0, tiled=True),
         lax.all_gather(attn_gate_weight, "sp", axis=0, tiled=True),
-        lax.all_gather(conv_gate_weight, "sp", axis=0, tiled=True),
+        gather_over(conv_gate_weight, "sp", 0),
     )
     stacked = jnp.concatenate(collected, axis=1)
 

time: 486 us -> 436 us (0.90)
  waiting for transfers between devices: 332 us -> 272 us
  starting transfers between devices: 11.4 us -> 19.7 us
    all_gather x1 -> x0, waiting for transfers between devices: 54.2 us -> none  [per_device(): lax.all_gather(conv_gate_weight, 'sp', axis=0, tiled=True)]
    all_to_all x0 -> x1, starting transfers between devices: none -> 8.34 us  [gather_over(): parts = lax.all_to_all(parts, axis, split_axis=0, concat_axis=0)]
  transfers between devices with their start and end apart: 13 -> 13, of which waited for: 8 -> 7; matrix products, arithmetic and copies ran while one was open for 7% -> 8% of each run, Pallas kernels for 0% -> 0%
where the time goes in v1:
time: 436 us; the launch traced here: 435 us
  waiting for transfers between devices  272 us (62%)
  blocking collectives  90.8 us (21%)
  local copies, waits for them, and re-layouts  22.1 us (5%)
  starting transfers between devices  19.7 us (5%)
  between operations  13.7 us (3%)
  matrix products  9.45 us (2%)
  other arithmetic  7.61 us (2%)
    all_gather x1, waiting for transfers between devices, per_device(): lax.all_gather(pre_weight, 'sp', axis=0, tiled=True)  54.4 us
    all_gather x1, waiting for transfers between devices, per_device(): lax.all_gather(attn_gate_weight, 'sp', axis=0, tiled=True)  54.3 us
    all_gather x1, waiting for transfers between devices, per_device(): lax.all_gather(post_weight, 'sp', axis=0, tiled=True)  54.2 us
    all_gather x1, waiting for transfers between devices, per_device(): lax.all_gather(attn_out_weight, 'sp', axis=1, tiled=True)  50.4 us
    all_gather x1, blocking collectives, per_device(): lax.all_gather(key_weight, 'sp', axis=0, tiled=True)  46.1 us
    all_gather x1, blocking collectives, per_device(): lax.all_gather(value_weight, 'sp', axis=0, tiled=True)  40.3 us
    all_gather x1, waiting for transfers between devices, per_device(): lax.all_gather(conv_out_weight, 'sp', axis=1, tiled=True)  35.7 us
    unnamed x7, local copies, waits for them, and re-layouts  13.4 us
  transfers between devices with their start and end apart: 13, of which 7 were waited for; matrix products, arithmetic and copies ran while one was open for 8% of the time, Pallas kernels for 0%

profile of v1, /device:TPU:0, one launch (start us, length us, event | category | flops | bytes accessed | tf_op | source)
XLA Modules:
  0.0 435.3 jit_solution(15340231496960105664)
XLA Ops:
  6.5 0.7 all-gather.8.cloned.1.call-update
  7.3 0.0 all-gather.10.cloned.1.call-start
  7.3 0.7 all-gather.10.cloned.1.call-update
  8.0 0.0 all-gather.12.cloned.1.call-start
  8.1 0.7 all-gather.12.cloned.1.call-update
  8.7 0.0 all-gather.14.cloned.1.call-start
  8.8 0.5 all-gather.14.cloned.1.call-update
  9.3 0.0 all-gather.16.cloned.1.call-start
  9.4 0.5 all-gather.16.cloned.1.call-update
  9.9 0.0 all-gather.20.cloned.1.call-start
  9.9 0.5 all-gather.20.cloned.1.call-update
  10.5 1.9 stack.2
  12.4 8.3 %all-to-all-start = ((bf16[16,64,512]{2,1,0:T(8,128)(2,1)}), bf16[16,64,512]{2,1,0:T(8,128)(2,1)S(1)}, u32[]{:S(2)}, u32[]{:S(2)}) async-start(bf16[16,64,512]{2,1,0:T(8,128)(2,1)} %stack.2), calls=%async_computation | async-start | bytes 2097152 | tf_op jit(solution)/shard_map/all_to_all | solution.py:15
  20.8 0.0 all-gather.18.cloned.1.call-start
  20.8 0.7 all-gather.18.cloned.1.call-update
  21.5 0.0 reduce-scatter.2.cloned.1.call-start
  21.6 1.0 fusion.4
  22.6 2.5 psum.7
  25.1 1.0 fusion.6
  26.1 1.3 broadcast_in_dim.27
  27.4 2.0 all_gather.30
  29.4 1.4 fusion.35
  30.8 0.8 fusion.27
  31.6 46.1 %all_gather.32 = bf16[1024,256]{1,0:T(8,128)(2,1)S(1)} all-gather(bf16[64,256]{1,0:T(8,128)(2,1)} %param.17), channel_id=1, replica_groups=mesh['sp'=16,'tp'=2] {'sp'}, dimensions={0}, use_global_device_ids=true | all-gather | bytes 557056 | tf_op jit(solution)/shard_map/all_gather | solution.py:107
  77.6 40.3 %all_gather.33 = bf16[1024,256]{1,0:T(8,128)(2,1)S(1)} all-gather(bf16[64,256]{1,0:T(8,128)(2,1)} %param.18), channel_id=1, replica_groups=mesh['sp'=16,'tp'=2] {'sp'}, dimensions={0}, use_global_device_ids=true | all-gather | bytes 557056 | tf_op jit(solution)/shard_map/all_gather | solution.py:108
  118.0 2.3 constant_dynamic-update-slice_fusion.7
  120.3 0.9 constant_dynamic-update-slice_fusion.6
  121.2 0.9 constant_dynamic-update-slice_fusion.5
  122.1 11.2 %all-gather.10.cloned.1.call-done = bf16[1024,512]{1,0:T(8,128)(2,1)} async-done(((bf16[64,512]{1,0:T(8,128)(2,1)}), bf16[1024,512]{1,0:T(8,128)(2,1)}) %all-gather.10.cloned.1.call-update) | async-done | bytes 1048592 | tf_op jit(solution)/shard_map/all_gather | solution.py:109
  133.3 2.3 constant_dynamic-update-slice_fusion.4
  135.6 54.4 %all-gather.12.cloned.1.call-done = bf16[1024,512]{1,0:T(8,128)(2,1)} async-done(((bf16[64,512]{1,0:T(8,128)(2,1)}), bf16[1024,512]{1,0:T(8,128)(2,1)}) %all-gather.12.cloned.1.call-update) | async-done | bytes 1048592 | tf_op jit(solution)/shard_map/all_gather | solution.py:110
  190.0 2.4 constant_dynamic-update-slice_fusion.3
  192.4 54.2 %all-gather.14.cloned.1.call-done = bf16[1024,512]{1,0:T(8,128)(2,1)} async-done(((bf16[64,512]{1,0:T(8,128)(2,1)}), bf16[1024,512]{1,0:T(8,128)(2,1)}) %all-gather.14.cloned.1.call-update) | async-done | bytes 1048592 | tf_op jit(solution)/shard_map/all_gather | solution.py:111
  246.6 2.3 constant_dynamic-update-slice_fusion.2
  248.9 54.3 %all-gather.16.cloned.1.call-done = bf16[1024,512]{1,0:T(8,128)(2,1)} async-done(((bf16[64,512]{1,0:T(8,128)(2,1)}), bf16[1024,512]{1,0:T(8,128)(2,1)}) %all-gather.16.cloned.1.call-update) | async-done | bytes 1048592 | tf_op jit(solution)/shard_map/all_gather | solution.py:112
  303.2 2.3 constant_dynamic-update-slice_fusion.1
  305.4 0.0 all-to-all-done
  305.5 1.1 constant_dynamic-update-slice_fusion
  306.5 4.2 fusion.36
  310.8 0.7 fusion.31
  311.5 3.3 collective-permute-start.2
  314.8 1.3 collective-permute-start.3
  316.1 0.7 fusion.32
  316.8 5.2 %collective-permute-start = (bf16[64,512]{1,0:T(8,128)(2,1)}, bf16[64,512]{1,0:T(8,128)(2,1)}, u32[]{:S(2)}, u32[]{:S(2)}) collective-permute-start(bf16[64,512]{1,0:T(8,128)(2,1)} %get-tuple-element.9), channel_id=1, source_target_pairs={{0,2},{2,4},{4,6},{6,8},{8,10},{10,12},{12,14},{14,16},{16,18},{18... | collective-permute-start | bytes 196616 | tf_op jit(solution)/shard_map/ppermute | solution.py:39
  322.0 1.3 collective-permute-start.1
  323.3 0.7 copy.21
  324.0 0.0 collective-permute-done.2
  324.1 35.7 %all-gather.20.cloned.1.call-done = bf16[512,1024]{0,1:T(8,128)(2,1)} async-done(((bf16[512,64]{0,1:T(8,128)(2,1)}), bf16[512,1024]{0,1:T(8,128)(2,1)}) %all-gather.20.cloned.1.call-update) | async-done | bytes 1048592 | tf_op jit(solution)/shard_map/all_gather | solution.py:159
  359.7 1.7 convolution_bitcast_fusion
  361.4 0.0 collective-permute-done
  361.5 1.0 pad_maximum_fusion.1
  362.5 0.1 copy.20
  362.6 0.1 copy.19
  362.7 1.3 fusion.37
  363.9 0.7 broadcast_maximum_fusion
  364.6 0.7 broadcast_in_dim.28
  365.3 0.2 fusion.30
  365.5 0.6 convolution_convert_fusion
  366.1 50.4 %all-gather.18.cloned.1.call-done = bf16[512,1024]{0,1:T(8,128)(2,1)} async-done(((bf16[512,64]{0,1:T(8,128)(2,1)}), bf16[512,1024]{0,1:T(8,128)(2,1)}) %all-gather.18.cloned.1.call-update) | async-done | bytes 1048592 | tf_op jit(solution)/shard_map/all_gather | solution.py:158
  416.4 1.7 convolution_bitcast_fusion.1
  418.2 1.1 pad_maximum_fusion
  419.2 0.0 reduce-scatter.2.cloned.1.call-update
  419.2 7.4 %reduce-scatter.2.cloned.1.call-done = f32[512,256]{0,1:T(8,128)} async-done(((f32[1024,256]{0,1:T(8,128)}), f32[512,256]{0,1:T(8,128)}) %reduce-scatter.2.cloned.1.call-update) | async-done | bytes 524304 | tf_op jit(solution)/shard_map/reduce_scatter | solution.py:47
  426.6 1.8 fusion.9
  (12 shorter events, 0.1 us)
Async XLA Ops:
  6.5 111.4 %all-gather.8.cloned.1.call-start = ((), (), s32[]{:S(2)}) async-start(), calls=%async_computation.2 | async-start | bytes 1114112 | tf_op jit(solution)/shard_map/all_gather | solution.py:106
  7.3 126.1 %all-gather.10.cloned.1.call-start = ((), (), s32[]{:S(2)}) async-start(), calls=%async_computation.3 | async-start | bytes 1114112 | tf_op jit(solution)/shard_map/all_gather | solution.py:109
  8.0 182.0 %all-gather.12.cloned.1.call-start = ((), (), s32[]{:S(2)}) async-start(), calls=%async_computation.4 | async-start | bytes 1114112 | tf_op jit(solution)/shard_map/all_gather | solution.py:110
  8.7 237.9 %all-gather.14.cloned.1.call-start = ((), (), s32[]{:S(2)}) async-start(), calls=%async_computation.5 | async-start | bytes 1114112 | tf_op jit(solution)/shard_map/all_gather | solution.py:111
  9.3 293.8 %all-gather.16.cloned.1.call-start = ((), (), s32[]{:S(2)}) async-start(), calls=%async_computation.6 | async-start | bytes 1114112 | tf_op jit(solution)/shard_map/all_gather | solution.py:112
  9.9 349.8 %all-gather.20.cloned.1.call-start = ((), (), s32[]{:S(2)}) async-start(), calls=%async_computation.8 | async-start | bytes 1114112 | tf_op jit(solution)/shard_map/all_gather | solution.py:159
  12.4 293.0 %all-to-all-start = ((bf16[16,64,512]{2,1,0:T(8,128)(2,1)}), bf16[16,64,512]{2,1,0:T(8,128)(2,1)S(1)}, u32[]{:S(2)}, u32[]{:S(2)}) async-start(bf16[16,64,512]{2,1,0:T(8,128)(2,1)} %stack.2), calls=%async_computation | async-start | bytes 2097152 | tf_op jit(solution)/shard_map/all_to_all | solution.py:15
  20.8 395.7 %all-gather.18.cloned.1.call-start = ((), (), s32[]{:S(2)}) async-start(), calls=%async_computation.7 | async-start | bytes 1114112 | tf_op jit(solution)/shard_map/all_gather | solution.py:158
  21.5 405.1 %reduce-scatter.2.cloned.1.call-start = ((), (), s32[]{:S(2)}) async-start(), calls=%async_computation.9 | async-start | bytes 1572864 | tf_op jit(solution)/shard_map/reduce_scatter | solution.py:47
  311.5 12.5 %collective-permute-start.2 = (bf16[1,512]{1,0:T(2,128)(2,1)S(1)}, bf16[1,512]{1,0:T(2,128)(2,1)S(1)}, u32[]{:S(2)}, u32[]{:S(2)}) collective-permute-start(bf16[1,512]{1,0:T(2,128)(2,1)S(1)} %get-tuple-element.13), channel_id=1, source_target_pairs={{0,2},{2,4},{4,6},{6,8},{8,10},{10,12},{12,14},{14,16},{16,18},{18... | collective-permute-start | bytes 3080 | tf_op jit(solution)/shard_map/ppermute | solution.py:39
  314.8 9.2 %collective-permute-start.3 = (bf16[1,512]{1,0:T(2,128)(2,1)S(1)}, bf16[1,512]{1,0:T(2,128)(2,1)S(1)}, u32[]{:S(2)}, u32[]{:S(2)}) collective-permute-start(bf16[1,512]{1,0:T(2,128)(2,1)S(1)} %get-tuple-element.14), channel_id=1, source_target_pairs={{2,0},{4,2},{6,4},{8,6},{10,8},{12,10},{14,12},{16,14},{18,16},{20... | collective-permute-start | bytes 3080 | tf_op jit(solution)/shard_map/ppermute | solution.py:40
  316.8 44.6 %collective-permute-start = (bf16[64,512]{1,0:T(8,128)(2,1)}, bf16[64,512]{1,0:T(8,128)(2,1)}, u32[]{:S(2)}, u32[]{:S(2)}) collective-permute-start(bf16[64,512]{1,0:T(8,128)(2,1)} %get-tuple-element.9), channel_id=1, source_target_pairs={{0,2},{2,4},{4,6},{6,8},{8,10},{10,12},{12,14},{14,16},{16,18},{18... | collective-permute-start | bytes 196616 | tf_op jit(solution)/shard_map/ppermute | solution.py:39
  322.0 39.5 %collective-permute-start.1 = (bf16[64,512]{1,0:T(8,128)(2,1)}, bf16[64,512]{1,0:T(8,128)(2,1)}, u32[]{:S(2)}, u32[]{:S(2)}) collective-permute-start(bf16[64,512]{1,0:T(8,128)(2,1)} %get-tuple-element.10), channel_id=1, source_target_pairs={{2,0},{4,2},{6,4},{8,6},{10,8},{12,10},{14,12},{16,14},{18,16},{20... | collective-permute-start | bytes 196616 | tf_op jit(solution)/shard_map/ppermute | solution.py:40
Sparse Core Ops, SparseCore 0:
  10.1 65.1 all-gather.7
  78.0 55.2 all-gather.9
  136.1 53.9 all-gather.11
  192.6 53.9 all-gather.13
  249.2 53.9 all-gather.15
  305.8 53.9 all-gather.19
  362.5 53.9 all-gather.17
  419.4 7.2 reduce-scatter.1
